TPU v7x, 128 devices: a whole 4x4x4 slice. The times are simulated.
128 devices in a mesh: gr: 2 (over z_hi), fs: 32 (over z_lo, y, x), tp: 2 (over core).
Axes of the slice: x: 4, y: 4, z: 4 (z_hi: 2, z_lo: 2; z = z_hi * 2 + z_lo), core: 2. Of those that a mesh axis runs over, the one named last changes fastest.
Arguments:
- tokens: bfloat16 [4, 2048, 2048], P(('gr', 'tp')), may hold values from -6 to 6
- gate_master: float32 [3, 2048, 7168], P(None, 'fs', ('gr', 'tp')), may hold values from -0.125 to 0.125
- up_master: float32 [3, 2048, 7168], P(None, 'fs', ('gr', 'tp')), may hold values from -0.125 to 0.125
- down_master: float32 [3, 7168, 2048], P(None, 'fs', ('gr', 'tp')), may hold values from -0.0625 to 0.0625
- norm_gain: float32 [2048], P('fs'), may hold values from 0.1 to 1.9
- route: int32 [4, 2048, 2], P(('gr', 'tp')), may hold values from 0 to 2, all different within a row
- route_weight: float32 [4, 2048, 2], P(('gr', 'tp')), may hold values from 0.05 to 1
Outputs:
- gate_out: bfloat16 [3, 2048, 7168], P(None, None, 'fs')
- up_out: bfloat16 [3, 2048, 7168], P(None, None, 'fs')
- down_out: bfloat16 [3, 7168, 2048], P(None, 'fs')
- mixed: bfloat16 [4, 2048, 2048], P(('gr', 'tp'), 'fs')
Inputs may be any that keep to these rules, and one draw needn't show every extreme that they name: `route`: each token names two different experts; every expert is named by some token.
All inputs are finite; a program needn't handle non-finite values.
Results may differ from a plain program's by a relative error of at most 0.024.
Values may be sent and summed in bfloat16 or wider, within the bound.
No kernel may reach another device: no remote copies, remote signals or barrier semaphores. Data moves between devices by JAX's collectives and lax.ppermute only.
A program may use at most 192 MiB of HBM per device.

v0:
```python
import jax
import jax.numpy as jnp
from jax import lax
from jax.sharding import Mesh
from jax.sharding import PartitionSpec as P

FS = ("fs_0", "fs_1", "fs_2")


def reduced_to_own(blocks, axes, order):
    dims = [lax.axis_size(a) for a in axes]
    blocks = blocks.reshape(*dims, *blocks.shape[1:])
    blocks = blocks.transpose(*order, *range(len(axes), blocks.ndim))
    blocks = blocks.reshape(-1, *blocks.shape[len(axes) :])
    for k in order:
        blocks = lax.psum_scatter(blocks, axes[k], scatter_dimension=0, tiled=True)
    return blocks[0]


def split_up(array, dim, peers):
    dims = array.shape
    blocks = array.reshape(*dims[:dim], peers, dims[dim] // peers, *dims[dim + 1 :])
    return jnp.moveaxis(blocks, dim, 0)


def sum_by_axis_2(array, axes, order, dim):
    peers = lax.axis_size(axes)
    return reduced_to_own(split_up(array, dim, peers), axes, order)


def normalize(rows_in):
    values = rows_in.astype(jnp.float32)
    scaled = values * lax.rsqrt(jnp.mean(values * values, axis=-1, keepdims=True) + 1e-06)
    return scaled.astype(jnp.bfloat16)


def mixing(chosen, weights, experts):
    share = weights / jnp.sum(weights, axis=-1, keepdims=True)
    labels = jnp.arange(experts, dtype=jnp.int32)
    match = (chosen[:, :, None] == labels[None, None, :]).astype(jnp.float32)
    return jnp.sum(share[:, :, None] * match, axis=1)


def expert_term(normed, mix_column, gate_weight, up_weight, down_weight):
    gate_act = jnp.dot(normed, gate_weight, preferred_element_type=jnp.float32)
    up_act = jnp.dot(normed, up_weight, preferred_element_type=jnp.float32)
    hidden = (jax.nn.silu(gate_act) * up_act).astype(jnp.bfloat16)
    projected = jnp.dot(hidden, down_weight, preferred_element_type=jnp.float32)
    return mix_column * projected


def shards(tokens, gate_master, up_master, down_master, norm_gain, route, route_weight):
    scaled_gain = norm_gain[None, :, None]
    gate_local = (scaled_gain * gate_master).astype(jnp.bfloat16)
    up_local = (scaled_gain * up_master).astype(jnp.bfloat16)
    down_local = down_master.astype(jnp.bfloat16)
    experts = gate_local.shape[0]
    normed = normalize(tokens[0])
    combine = mixing(route[0], route_weight[0], experts)
    width = normed.shape[1]
    gate_rows, up_rows, down_out = (
        lax.all_gather(gate_local, ("gr", "tp"), axis=2, tiled=True),
        lax.all_gather(up_local, ("gr", "tp"), axis=2, tiled=True),
        lax.all_gather(down_local, ("gr", "tp"), axis=2, tiled=True),
    )
    gate_out, up_out = (
        lax.all_to_all(gate_rows, FS, split_axis=2, concat_axis=1, tiled=True),
        lax.all_to_all(up_rows, FS, split_axis=2, concat_axis=1, tiled=True),
    )
    own_rows = normed.shape[0] // lax.axis_size(FS)
    total = jnp.zeros((own_rows * lax.axis_size(FS), width), jnp.float32)
    for index in range(experts):
        total = total + expert_term(
            normed, combine[:, index : index + 1], gate_out[index], up_out[index], down_out[index]
        )
    summed = sum_by_axis_2(total.astype(jnp.bfloat16), FS, (1, 2, 0), 0).astype(jnp.float32)
    mixed = summed.astype(jnp.bfloat16)[None]
    return (gate_out, up_out, down_out, mixed)


def solution(mesh):
    split = Mesh(
        mesh.devices.reshape(mesh.shape["gr"], 2, 4, 4, mesh.shape["tp"]),
        ("gr", "fs_0", "fs_1", "fs_2", "tp"),
    )
    in_specs = (
        P(("gr", "tp"), None, None),
        P(None, FS, ("gr", "tp")),
        P(None, FS, ("gr", "tp")),
        P(None, FS, ("gr", "tp")),
        P(FS),
        P(("gr", "tp"), None, None),
        P(("gr", "tp"), None, None),
    )
    out_specs = (P(None, None, FS), P(None, None, FS), P(None, FS, None), P(("gr", "tp"), FS, None))
    return jax.shard_map(
        shards, mesh=split, in_specs=in_specs, out_specs=out_specs, check_vma=False
    )
```

profile of v0, /device:TPU:1, one launch (start us, length us, event | category | flops | bytes accessed | tf_op | source)
XLA Modules:
  0.0 390.9 jit_solution(5299467397481243480)
XLA Ops:
  7.2 3.1 multiply_convert_fusion
  11.1 33.5 %all-gather.4.cloned.1.call-done = bf16[3,64,7168]{2,1,0:T(8,128)(2,1)} async-done(((bf16[3,64,1792]{2,1,0:T(8,128)(2,1)}), bf16[3,64,7168]{2,1,0:T(8,128)(2,1)}) %all-gather.4.cloned.1.call-update) | async-done | bytes 2752528 | tf_op jit(solution)/shard_map/all_gather | solution.py:62
  44.5 10.1 %copy.41 = bf16[3,64,7168]{1,0,2:T(4,128)(2,1)} copy(bf16[3,64,7168]{2,1,0:T(8,128)(2,1)} %all-gather.4.cloned.1.call-done) | data formatting | bytes 5505024 | tf_op jit(solution)/shard_map/all_gather | solution.py:62
  54.6 12.6 %reshape.105 = bf16[32,2,21504]{2,1,0:T(2,128)(2,1)} reshape(bf16[7168,3,64]{2,1,0:T(4,128)(2,1)} %bitcast.55) | data formatting | bytes 5505024
  67.2 7.0 %all-to-all-start = ((bf16[32,2,21504]{2,1,0:T(2,128)(2,1)}), bf16[32,2,21504]{2,1,0:T(2,128)(2,1)S(1)}, u32[]{:S(2)}, u32[]{:S(2)}) async-start(bf16[32,2,21504]{2,1,0:T(2,128)(2,1)} %reshape.105), calls=%async_computation | async-start | bytes 5505024 | tf_op jit(solution)/shard_map/all_to_all | solution.py:67
  74.3 2.3 convert_element_type.47
  76.7 10.1 %copy.43 = bf16[3,64,7168]{1,0,2:T(4,128)(2,1)} copy(bf16[3,64,7168]{2,1,0:T(8,128)(2,1)} %all-gather.6.cloned.1.call-done) | data formatting | bytes 5505024 | tf_op jit(solution)/shard_map/all_gather | solution.py:63
  86.8 12.6 %reshape.107 = bf16[32,2,21504]{2,1,0:T(2,128)(2,1)} reshape(bf16[7168,3,64]{2,1,0:T(4,128)(2,1)} %bitcast.56) | data formatting | bytes 5505024
  99.4 9.2 %all-to-all-done = bf16[32,2,21504]{2,1,0:T(2,128)(2,1)S(1)} async-done(((bf16[32,2,21504]{2,1,0:T(2,128)(2,1)}), bf16[32,2,21504]{2,1,0:T(2,128)(2,1)S(1)}, u32[]{:S(2)}, u32[]{:S(2)}) %all-to-all-start) | async-done | bytes 2752544 | tf_op jit(solution)/shard_map/all_to_all | solution.py:67
  108.6 6.3 %all-to-all-start.1 = ((bf16[32,2,21504]{2,1,0:T(2,128)(2,1)}), bf16[32,2,21504]{2,1,0:T(2,128)(2,1)}, u32[]{:S(2)}, u32[]{:S(2)}) async-start(bf16[32,2,21504]{2,1,0:T(2,128)(2,1)} %reshape.107), calls=%async_computation.1 | async-start | bytes 5505024 | tf_op jit(solution)/shard_map/all_to_all | solution.py:68
  115.1 5.1 %fusion = f32[2048]{0:T(1024)S(1)} fusion(bf16[1,2048,2048]{2,1,0:T(8,128)(2,1)} %param.7), kind=kLoop, calls=%fused_computation.2 | loop fusion | flops 12580864 | bytes 8396800 | tf_op jit(solution)/shard_map/reduce_sum | solution.py:33
  120.3 8.0 %fusion.2 = bf16[2048,2048]{1,0:T(8,128)(2,1)} fusion(bf16[1,2048,2048]{2,1,0:T(8,128)(2,1)} %param.7, f32[2048]{0:T(1024)S(1)} %add_rsqrt_fusion), kind=kLoop, calls=%fused_computation.5 | loop fusion | flops 12582912 | bytes 16785408 | tf_op jit(solution)/shard_map/convert_element_type | solution.py:34
  128.3 8.7 %reshape.106 = bf16[7168,3,64]{2,1,0:T(4,128)(2,1)} reshape(bf16[32,2,21504]{2,1,0:T(2,128)(2,1)S(1)} %all-to-all-done) | data formatting | bytes 5505024
  136.9 10.7 %copy.42 = bf16[3,64,32,224]{3,1,2,0:T(8,128)(2,1)S(1)} copy(bf16[3,64,32,224]{1,0,3,2:T(4,128)(2,1)} %bitcast.57) | data formatting | bytes 5505024 | tf_op jit(solution)/shard_map/all_to_all | solution.py:67
  147.7 0.9 all-to-all-done.1
  148.6 12.5 %reshape.108 = bf16[7168,3,64]{2,1,0:T(4,128)(2,1)} reshape(bf16[32,2,21504]{2,1,0:T(2,128)(2,1)} %all-to-all-done.1) | data formatting | bytes 5505024
  161.0 11.4 %copy.44 = bf16[3,64,32,224]{3,1,2,0:T(8,128)(2,1)} copy(bf16[3,64,32,224]{1,0,3,2:T(4,128)(2,1)} %bitcast.58) | data formatting | bytes 5505024 | tf_op jit(solution)/shard_map/all_to_all | solution.py:68
  172.6 1.7 copy-done
  174.3 1.8 fusion.25
  176.1 8.0 %fusion.27 = f32[2048,224]{0,1:T(8,128)} fusion(bf16[2048,2048]{1,0:T(8,128)(2,1)} %fusion.2, bf16[2048,224]{1,0:T(8,128)(2,1)S(1)} %bitcast.68), kind=kOutput, calls=%fused_computation.41 | convolution fusion | flops 1879048192 | bytes 11141120 | tf_op jit(solution)/shard_map/dot_general | solution.py:45
  184.1 4.0 %fusion.28 = f32[2048,224]{0,1:T(8,128)} fusion(bf16[2048,2048]{1,0:T(8,128)(2,1)S(1)} %bitcast.52, bf16[2048,224]{1,0:T(8,128)(2,1)S(1)} %bitcast.67), kind=kOutput, calls=%fused_computation.42 | convolution fusion | flops 1879048192 | bytes 11141120 | tf_op jit(solution)/shard_map/dot_general | solution.py:45
  188.1 4.0 %fusion.29 = f32[2048,224]{0,1:T(8,128)} fusion(bf16[2048,2048]{1,0:T(8,128)(2,1)S(1)} %bitcast.52, bf16[2048,224]{1,0:T(8,128)(2,1)S(1)} %bitcast.66), kind=kOutput, calls=%fused_computation.43 | convolution fusion | flops 1879048192 | bytes 11141120 | tf_op jit(solution)/shard_map/dot_general | solution.py:45
  192.1 15.3 %fusion.7 = f32[2048,2048]{1,0:T(8,128)} fusion(bf16[2048,2048]{1,0:T(8,128)(2,1)} %fusion.2, bf16[2048,224]{1,0:T(8,128)(2,1)} %bitcast.64, f32[2048,224]{0,1:T(8,128)} %fusion.27, bf16[3,224,2048]{2,1,0:T(8,128)(2,1)} %all-gather.8.cloned.1.call-done), kind=kOutput, calls=%fused_computation.13 | convolution fusion | flops 3760848896 | bytes 28966912 | tf_op jit(solution)/shard_map/dot_general | solution.py:48
  207.4 15.5 %fusion.6 = f32[2048,2048]{1,0:T(8,128)} fusion(bf16[2048,2048]{1,0:T(8,128)(2,1)} %fusion.2, bf16[2048,224]{1,0:T(8,128)(2,1)} %bitcast.63, f32[2048,224]{0,1:T(8,128)} %fusion.28, bf16[3,224,2048]{2,1,0:T(8,128)(2,1)} %all-gather.8.cloned.1.call-done), kind=kOutput, calls=%fused_computation.12 | convolution fusion | flops 3760848896 | bytes 28966912 | tf_op jit(solution)/shard_map/dot_general | solution.py:48
  222.9 19.2 %add_convert_fusion = bf16[2048,2048]{1,0:T(8,128)(2,1)} fusion(f32[2048,2048]{1,0:T(8,128)} %fusion.6, f32[2048,2048]{1,0:T(8,128)} %fusion.7, f32[2048]{0:T(1024)S(1)} %bitcast.70, f32[2048]{0:T(1024)S(1)} %bitcast.71, f32[2048]{0:T(1024)S(1)} %bitcast.69, bf16[3,224,2048]{2,1,0:T(8,128)(2,1)} %all-gather.8.cloned.1.call-done, ...), kind=kOutput, calls=%fused_computation.4 | convolution fusion | flops 3786014720 | bytes 54157312 | tf_op jit(solution)/shard_map/dot_general | solution.py:48
  242.0 8.3 %copy.45 = bf16[4,4,2,64,2048]{4,3,2,1,0:T(8,128)(2,1)} copy(bf16[4,4,2,64,2048]{4,3,1,0,2:T(8,128)(2,1)} %bitcast.54) | data formatting | bytes 16777216 | tf_op jit(solution)/shard_map/transpose | solution.py:13
  250.4 80.8 %reduce-scatter.4.cloned.1.call-done = bf16[8,64,2048]{2,1,0:T(8,128)(2,1)} async-done(((bf16[32,64,2048]{2,1,0:T(8,128)(2,1)}), bf16[8,64,2048]{2,1,0:T(8,128)(2,1)}) %reduce-scatter.4.cloned.1.call-update) | async-done | bytes 2097168 | tf_op jit(solution)/shard_map/reduce_scatter | solution.py:16
  331.3 31.6 %reduce-scatter.6.cloned.1.call-done = bf16[2,64,2048]{2,1,0:T(8,128)(2,1)} async-done(((bf16[8,64,2048]{2,1,0:T(8,128)(2,1)}), bf16[2,64,2048]{2,1,0:T(8,128)(2,1)}) %reduce-scatter.6.cloned.1.call-update) | async-done | bytes 524304 | tf_op jit(solution)/shard_map/reduce_scatter | solution.py:16
  362.9 2.7 copy.46
  365.6 4.7 %copy.47 = bf16[3,2048,224]{1,2,0:T(8,128)(2,1)} copy(bf16[3,2048,224]{2,1,0:T(8,128)(2,1)} %bitcast.61) | data formatting | bytes 5505024
  370.3 12.2 %reduce-scatter.8.cloned.1.call-done = bf16[1,64,2048]{2,1,0:T(8,128)(2,1)} async-done(((bf16[2,64,2048]{2,1,0:T(8,128)(2,1)}), bf16[1,64,2048]{2,1,0:T(8,128)(2,1)}) %reduce-scatter.8.cloned.1.call-update) | async-done | bytes 262160 | tf_op jit(solution)/shard_map/reduce_scatter | solution.py:16
  382.5 1.5 copy.49
  (32 shorter events, 1.4 us)
Async XLA Ops:
  7.2 37.4 %all-gather.4.cloned.1.call-start = ((), (), s32[]{:S(2)}) async-start(), calls=%async_computation.5 | async-start | bytes 3440640 | tf_op jit(solution)/shard_map/all_gather | solution.py:62
  10.3 66.4 %all-gather.6.cloned.1.call-start = ((), (), s32[]{:S(2)}) async-start(), calls=%async_computation.6 | async-start | bytes 3440640 | tf_op jit(solution)/shard_map/all_gather | solution.py:63
  67.2 41.4 %all-to-all-start = ((bf16[32,2,21504]{2,1,0:T(2,128)(2,1)}), bf16[32,2,21504]{2,1,0:T(2,128)(2,1)S(1)}, u32[]{:S(2)}, u32[]{:S(2)}) async-start(bf16[32,2,21504]{2,1,0:T(2,128)(2,1)} %reshape.105), calls=%async_computation | async-start | bytes 5505024 | tf_op jit(solution)/shard_map/all_to_all | solution.py:67
  74.3 2.4 copy-start.2
  74.3 117.9 %all-gather.8.cloned.1.call-start = ((), (), s32[]{:S(2)}) async-start(), calls=%async_computation.7 | async-start | bytes 3440640 | tf_op jit(solution)/shard_map/all_gather | solution.py:64
  99.4 15.6 %copy-start.3 = (s32[1,2048,2]{1,2,0:T(2,128)S(1)}, s32[1,2048,2]{1,2,0:T(2,128)}, u32[]{:S(2)}) copy-start(s32[1,2048,2]{1,2,0:T(2,128)} %param.12) | copy-start | bytes 49156
  108.6 39.9 %all-to-all-start.1 = ((bf16[32,2,21504]{2,1,0:T(2,128)(2,1)}), bf16[32,2,21504]{2,1,0:T(2,128)(2,1)}, u32[]{:S(2)}, u32[]{:S(2)}) async-start(bf16[32,2,21504]{2,1,0:T(2,128)(2,1)} %reshape.107), calls=%async_computation.1 | async-start | bytes 5505024 | tf_op jit(solution)/shard_map/all_to_all | solution.py:68
  115.0 216.3 %reduce-scatter.4.cloned.1.call-start = ((), (), s32[]{:S(2)}) async-start(), calls=%async_computation.8 | async-start | bytes 10485760 | tf_op jit(solution)/shard_map/reduce_scatter | solution.py:16
  172.4 1.9 copy-start
  174.3 9.8 %slice-start = ((s8[8388608]{0:T(1024)(128)(4,1)}), s8[4194304]{0:T(1024)(128)(4,1)S(1)}, s32[]{:S(2)}) async-start(s8[8388608]{0:T(1024)(128)(4,1)} %bitcast.51), calls=%async_computation.11 | async-start | bytes 8388608
  176.1 8.0 %slice-start.1 = ((s8[8388608]{0:T(1024)(128)(4,1)}), s8[4194304]{0:T(1024)(128)(4,1)S(1)}, s32[]{:S(2)}) async-start(s8[8388608]{0:T(1024)(128)(4,1)} %bitcast.51), calls=%async_computation.12 | async-start | bytes 8388608
  250.3 112.5 %reduce-scatter.6.cloned.1.call-start = ((), (), s32[]{:S(2)}) async-start(), calls=%async_computation.9 | async-start | bytes 2621440 | tf_op jit(solution)/shard_map/reduce_scatter | solution.py:16
  331.2 51.3 %reduce-scatter.8.cloned.1.call-start = ((), (), s32[]{:S(2)}) async-start(), calls=%async_computation.10 | async-start | bytes 786432 | tf_op jit(solution)/shard_map/reduce_scatter | solution.py:16
  365.6 16.9 %copy-start.1 = (bf16[3,224,2048]{2,1,0:T(8,128)(2,1)S(1)}, bf16[3,224,2048]{2,1,0:T(8,128)(2,1)}, u32[]{:S(2)}) copy-start(bf16[3,224,2048]{2,1,0:T(8,128)(2,1)} %all-gather.8.cloned.1.call-done) | copy-start | bytes 8257540
Sparse Core Ops, SparseCore 0:
  10.4 34.0 all-gather.3
  46.8 29.6 all-gather.5
  78.1 74.4 all-gather.7
  250.5 80.7 reduce-scatter.3
  333.5 29.3 reduce-scatter.5
  365.6 16.8 reduce-scatter.7
where the time goes:
time: 393 us; the launch traced here: 391 us
  waiting for transfers between devices  169 us (43%)
  local copies, waits for them, and re-layouts  110 us (28%)
  matrix products  65.9 us (17%)
  other arithmetic  18.6 us (5%)
  between operations  14.2 us (4%)
  starting transfers between devices  13.6 us (3%)
    reduce_scatter x3, waiting for transfers between devices, reduced_to_own(): blocks = lax.psum_scatter(blocks, axes[k], scatter_dimension=0, tiled=True)  125 us
    unnamed x19, local copies, waits for them, and re-layouts  57 us
    dot_general x3, matrix products, expert_term(): projected = jnp.dot(hidden, down_weight, preferred_element_type=jnp.float32)  49.9 us
    all_gather x1, waiting for transfers between devices, shards(): lax.all_gather(gate_local, ('gr', 'tp'), axis=2, tiled=True)  33.5 us
    dot_general x3, matrix products, expert_term(): gate_act = jnp.dot(normed, gate_weight, preferred_element_type=jnp.float32)  16 us
    all_to_all x1, local copies, waits for them, and re-layouts, shards(): lax.all_to_all(up_rows, FS, split_axis=2, concat_axis=1, tiled=True)  11.4 us
    all_to_all x1, local copies, waits for them, and re-layouts, shards(): lax.all_to_all(gate_rows, FS, split_axis=2, concat_axis=1, tiled=True)  10.7 us
    all_gather x1, local copies, waits for them, and re-layouts, shards(): lax.all_gather(up_local, ('gr', 'tp'), axis=2, tiled=True)  10.1 us
  transfers between devices with their start and end apart: 8, of which 6 were waited for; matrix products, arithmetic and copies ran while one was open for 33% of the time, Pallas kernels for 0%

commit v1 on v0

--- a/solution.py
+++ b/solution.py
@@ -59,7 +59,12 @@
     combine = mixing(route[0], route_weight[0], experts)
     width = normed.shape[1]
     gate_rows, up_rows, down_out = (
-        lax.all_gather(gate_local, ("gr", "tp"), axis=2, tiled=True),
+        jnp.concatenate(
+            lax.all_to_all(
+                jnp.stack(lax.axis_size(("gr", "tp")) * [gate_local], 0), ("gr", "tp"), 0, 0
+            ),
+            axis=2,
+        ),
         lax.all_gather(up_local, ("gr", "tp"), axis=2, tiled=True),
         lax.all_gather(down_local, ("gr", "tp"), axis=2, tiled=True),
     )

time: 393 us -> 401 us (1.020)
  local copies, waits for them, and re-layouts: 110 us -> 119 us
  waiting for transfers between devices: 169 us -> 160 us
  starting transfers between devices: 13.6 us -> 22.5 us
    all_to_all x0 -> x1, waiting for transfers between devices: none -> 45.6 us  [shards(): lax.all_to_all(jnp.stack(lax.axis_size(('gr', 'tp')) * [gate_local], 0),...]
    all_gather x1 -> x0, waiting for transfers between devices: 33.5 us -> none  [shards(): lax.all_gather(gate_local, ('gr', 'tp'), axis=2, tiled=True)]
    reduce_scatter x3, waiting for transfers between devices: 125 us -> 114 us  [reduced_to_own(): blocks = lax.psum_scatter(blocks, axes[k], scatter_dimension=0, tiled=True)]
    all_gather x1 -> x0, local copies, waits for them, and re-layouts: 10.1 us -> none  [shards(): lax.all_gather(gate_local, ('gr', 'tp'), axis=2, tiled=True)]
    all_to_all x1, waiting for transfers between devices: 9.23 us -> 0.01 us  [shards(): lax.all_to_all(gate_rows, FS, split_axis=2, concat_axis=1, tiled=True)]
    all_to_all x1 -> x2, local copies, waits for them, and re-layouts: 10.7 us -> 19.4 us  [shards(): lax.all_to_all(gate_rows, FS, split_axis=2, concat_axis=1, tiled=True)]
    reshape x0 -> x1, local copies, waits for them, and re-layouts: none -> 7.43 us  [shards(): jnp.concatenate(lax.all_to_all(jnp.stack(lax.axis_size(('gr', 'tp')) * [g...]
    all_to_all x0 -> x1, starting transfers between devices: none -> 6.64 us  [shards(): lax.all_to_all(jnp.stack(lax.axis_size(('gr', 'tp')) * [gate_local], 0),...]
  transfers between devices with their start and end apart: 8 -> 8, of which waited for: 6 -> 4; matrix products, arithmetic and copies ran while one was open for 33% -> 35% of each run, Pallas kernels for 0% -> 0%
where the time goes in v1:
time: 401 us; the launch traced here: 399 us
  waiting for transfers between devices  160 us (40%)
  local copies, waits for them, and re-layouts  119 us (30%)
  matrix products  65.4 us (16%)
  starting transfers between devices  22.5 us (6%)
  other arithmetic  18.4 us (5%)
  between operations  13.9 us (3%)
    reduce_scatter x3, waiting for transfers between devices, reduced_to_own(): blocks = lax.psum_scatter(blocks, axes[k], scatter_dimension=0, tiled=True)  114 us
    unnamed x15, local copies, waits for them, and re-layouts  57.2 us
    dot_general x3, matrix products, expert_term(): projected = jnp.dot(hidden, down_weight, preferred_element_type=jnp.float32)  49.6 us
    all_to_all x1, waiting for transfers between devices, shards(): lax.all_to_all(jnp.stack(lax.axis_size(('gr', 'tp')) * [gate_local], 0),...  45.6 us
    all_to_all x2, local copies, waits for them, and re-layouts, shards(): lax.all_to_all(gate_rows, FS, split_axis=2, concat_axis=1, tiled=True)  19.4 us
    dot_general x3, matrix products, expert_term(): gate_act = jnp.dot(normed, gate_weight, preferred_element_type=jnp.float32)  15.7 us
    all_to_all x1, local copies, waits for them, and re-layouts, shards(): lax.all_to_all(up_rows, FS, split_axis=2, concat_axis=1, tiled=True)  10.9 us
    all_gather x1, local copies, waits for them, and re-layouts, shards(): lax.all_gather(up_local, ('gr', 'tp'), axis=2, tiled=True)  10 us
  transfers between devices with their start and end apart: 8, of which 4 were waited for; matrix products, arithmetic and copies ran while one was open for 35% of the time, Pallas kernels for 0%

profile of v1, /device:TPU:1, one launch (start us, length us, event | category | flops | bytes accessed | tf_op | source)
XLA Modules:
  0.0 399.0 jit_solution(12961590832164350112)
XLA Ops:
  7.2 2.9 multiply_convert_fusion
  10.1 1.8 stack.2
  11.9 6.6 %all-to-all-start = ((bf16[4,3,64,1792]{3,2,1,0:T(8,128)(2,1)}), bf16[4,3,64,1792]{3,2,1,0:T(8,128)(2,1)S(1)}, u32[]{:S(2)}, u32[]{:S(2)}) async-start(bf16[4,3,64,1792]{3,2,1,0:T(8,128)(2,1)} %stack.2), calls=%async_computation | async-start | bytes 5505024 | tf_op jit(solution)/shard_map/all_to_all | solution.py:63
  18.5 2.3 convert_element_type.47
  20.9 45.6 %all-to-all-done = bf16[4,3,64,1792]{3,2,1,0:T(8,128)(2,1)S(1)} async-done(((bf16[4,3,64,1792]{3,2,1,0:T(8,128)(2,1)}), bf16[4,3,64,1792]{3,2,1,0:T(8,128)(2,1)S(1)}, u32[]{:S(2)}, u32[]{:S(2)}) %all-to-all-start) | async-done | bytes 2752544 | tf_op jit(solution)/shard_map/all_to_all | solution.py:63
  66.5 7.4 %copy.67 = bf16[3,64,4,1792]{1,0,3,2:T(4,128)(2,1)} copy(bf16[3,64,4,1792]{3,1,0,2:T(8,128)(2,1)S(1)} %bitcast.67) | data formatting | bytes 5505024 | tf_op jit(solution)/shard_map/reshape | solution.py:62
  73.9 12.6 %reshape.115 = bf16[32,2,21504]{2,1,0:T(2,128)(2,1)} reshape(bf16[7168,3,64]{2,1,0:T(4,128)(2,1)} %bitcast.60) | data formatting | bytes 5505024
  86.5 7.7 %all-to-all-start.1 = ((bf16[32,2,21504]{2,1,0:T(2,128)(2,1)}), bf16[32,2,21504]{2,1,0:T(2,128)(2,1)S(1)}, u32[]{:S(2)}, u32[]{:S(2)}) async-start(bf16[32,2,21504]{2,1,0:T(2,128)(2,1)} %reshape.115), calls=%async_computation.1 | async-start | bytes 5505024 | tf_op jit(solution)/shard_map/all_to_all | solution.py:72
  94.3 5.1 %fusion = f32[2048]{0:T(1024)S(1)} fusion(bf16[1,2048,2048]{2,1,0:T(8,128)(2,1)} %param.7), kind=kLoop, calls=%fused_computation.2 | loop fusion | flops 12580864 | bytes 8396800 | tf_op jit(solution)/shard_map/reduce_sum | solution.py:33
  99.4 8.0 %fusion.2 = bf16[2048,2048]{1,0:T(8,128)(2,1)} fusion(bf16[1,2048,2048]{2,1,0:T(8,128)(2,1)} %param.7, f32[2048]{0:T(1024)S(1)} %add_rsqrt_fusion), kind=kLoop, calls=%fused_computation.5 | loop fusion | flops 12582912 | bytes 16785408 | tf_op jit(solution)/shard_map/convert_element_type | solution.py:34
  107.4 10.0 %copy.59 = bf16[3,64,7168]{1,0,2:T(4,128)(2,1)} copy(bf16[3,64,7168]{2,1,0:T(8,128)(2,1)} %all-gather.3.cloned.1.call-done) | data formatting | bytes 5505024 | tf_op jit(solution)/shard_map/all_gather | solution.py:68
  117.4 12.6 %reshape.117 = bf16[32,2,21504]{2,1,0:T(2,128)(2,1)} reshape(bf16[7168,3,64]{2,1,0:T(4,128)(2,1)} %bitcast.61) | data formatting | bytes 5505024
  130.0 7.9 %all-to-all-start.2 = ((bf16[32,2,21504]{2,1,0:T(2,128)(2,1)}), bf16[32,2,21504]{2,1,0:T(2,128)(2,1)}, u32[]{:S(2)}, u32[]{:S(2)}) async-start(bf16[32,2,21504]{2,1,0:T(2,128)(2,1)} %reshape.117), calls=%async_computation.2 | async-start | bytes 5505024 | tf_op jit(solution)/shard_map/all_to_all | solution.py:73
  138.1 8.7 %reshape.116 = bf16[7168,3,64]{2,1,0:T(4,128)(2,1)} reshape(bf16[32,2,21504]{2,1,0:T(2,128)(2,1)S(1)} %all-to-all-done.1) | data formatting | bytes 5505024
  146.8 8.1 %copy.68 = bf16[3,64,32,224]{3,2,1,0:T(8,128)(2,1)S(1)} copy(bf16[3,64,32,224]{1,0,3,2:T(4,128)(2,1)} %bitcast.56) | data formatting | bytes 5505024 | tf_op jit(solution)/shard_map/all_to_all | solution.py:72
  157.0 7.7 %fusion.29 = f32[2048,224]{0,1:T(8,128)} fusion(bf16[2048,2048]{1,0:T(8,128)(2,1)} %fusion.2, bf16[2048,224]{1,0:T(8,128)(2,1)S(1)} %bitcast.71), kind=kOutput, calls=%fused_computation.43 | convolution fusion | flops 1879048192 | bytes 11141120 | tf_op jit(solution)/shard_map/dot_general | solution.py:45
  164.7 4.0 %fusion.28 = f32[2048,224]{0,1:T(8,128)} fusion(bf16[2048,2048]{1,0:T(8,128)(2,1)S(1)} %bitcast.55, bf16[2048,224]{1,0:T(8,128)(2,1)S(1)} %bitcast.72), kind=kOutput, calls=%fused_computation.42 | convolution fusion | flops 1879048192 | bytes 11141120 | tf_op jit(solution)/shard_map/dot_general | solution.py:45
  168.7 4.0 %fusion.27 = f32[2048,224]{0,1:T(8,128)} fusion(bf16[2048,2048]{1,0:T(8,128)(2,1)S(1)} %bitcast.55, bf16[2048,224]{1,0:T(8,128)(2,1)S(1)} %bitcast.73), kind=kOutput, calls=%fused_computation.41 | convolution fusion | flops 1879048192 | bytes 11141120 | tf_op jit(solution)/shard_map/dot_general | solution.py:45
  172.7 12.5 %reshape.118 = bf16[7168,3,64]{2,1,0:T(4,128)(2,1)} reshape(bf16[32,2,21504]{2,1,0:T(2,128)(2,1)} %all-to-all-done.2) | data formatting | bytes 5505024
  185.2 10.9 %copy.60 = bf16[3,64,32,224]{3,1,2,0:T(8,128)(2,1)S(1)} copy(bf16[3,64,32,224]{1,0,3,2:T(4,128)(2,1)} %bitcast.62) | data formatting | bytes 5505024 | tf_op jit(solution)/shard_map/all_to_all | solution.py:73
  196.1 1.8 fusion.25
  197.9 15.2 %fusion.7 = f32[2048,2048]{1,0:T(8,128)} fusion(bf16[2048,2048]{1,0:T(8,128)(2,1)} %fusion.2, bf16[2048,224]{1,0:T(8,128)(2,1)} %bitcast.69, f32[2048,224]{0,1:T(8,128)} %fusion.27, bf16[3,224,2048]{2,1,0:T(8,128)(2,1)} %all-gather.5.cloned.1.call-done), kind=kOutput, calls=%fused_computation.13 | convolution fusion | flops 3760848896 | bytes 28966912 | tf_op jit(solution)/shard_map/dot_general | solution.py:48
  213.2 15.2 %fusion.6 = f32[2048,2048]{1,0:T(8,128)} fusion(bf16[2048,2048]{1,0:T(8,128)(2,1)} %fusion.2, bf16[2048,224]{1,0:T(8,128)(2,1)} %bitcast.68, f32[2048,224]{0,1:T(8,128)} %fusion.28, bf16[3,224,2048]{2,1,0:T(8,128)(2,1)} %all-gather.5.cloned.1.call-done), kind=kOutput, calls=%fused_computation.12 | convolution fusion | flops 3760848896 | bytes 28966912 | tf_op jit(solution)/shard_map/dot_general | solution.py:48
  228.4 19.2 %add_convert_fusion = bf16[2048,2048]{1,0:T(8,128)(2,1)} fusion(f32[2048,2048]{1,0:T(8,128)} %fusion.6, f32[2048,2048]{1,0:T(8,128)} %fusion.7, f32[2048]{0:T(1024)S(1)} %bitcast.75, f32[2048]{0:T(1024)S(1)} %bitcast.76, f32[2048]{0:T(1024)S(1)} %bitcast.74, bf16[3,224,2048]{2,1,0:T(8,128)(2,1)} %all-gather.5.cloned.1.call-done, ...), kind=kOutput, calls=%fused_computation.4 | convolution fusion | flops 3786014720 | bytes 54157312 | tf_op jit(solution)/shard_map/dot_general | solution.py:48
  247.6 8.3 %copy.64 = bf16[4,4,2,64,2048]{4,3,2,1,0:T(8,128)(2,1)} copy(bf16[4,4,2,64,2048]{4,3,1,0,2:T(8,128)(2,1)} %bitcast.59) | data formatting | bytes 16777216 | tf_op jit(solution)/shard_map/transpose | solution.py:13
  255.9 81.5 %reduce-scatter.4.cloned.1.call-done = bf16[8,64,2048]{2,1,0:T(8,128)(2,1)} async-done(((bf16[32,64,2048]{2,1,0:T(8,128)(2,1)}), bf16[8,64,2048]{2,1,0:T(8,128)(2,1)}) %reduce-scatter.4.cloned.1.call-update) | async-done | bytes 2097168 | tf_op jit(solution)/shard_map/reduce_scatter | solution.py:16
  337.5 31.6 %reduce-scatter.6.cloned.1.call-done = bf16[2,64,2048]{2,1,0:T(8,128)(2,1)} async-done(((bf16[8,64,2048]{2,1,0:T(8,128)(2,1)}), bf16[2,64,2048]{2,1,0:T(8,128)(2,1)}) %reduce-scatter.6.cloned.1.call-update) | async-done | bytes 524304 | tf_op jit(solution)/shard_map/reduce_scatter | solution.py:16
  369.1 11.4 %copy.69 = bf16[3,64,32,224]{3,1,2,0:T(8,128)(2,1)} copy(bf16[3,64,32,224]{1,0,3,2:T(4,128)(2,1)} %bitcast.57) | data formatting | bytes 5505024 | tf_op jit(solution)/shard_map/all_to_all | solution.py:72
  380.5 4.6 %copy.65 = bf16[3,2048,224]{1,2,0:T(8,128)(2,1)} copy(bf16[3,2048,224]{2,1,0:T(8,128)(2,1)} %bitcast.66) | data formatting | bytes 5505024
  385.1 2.7 copy.66
  387.7 1.1 reduce-scatter.8.cloned.1.call-done
  388.8 3.7 copy.72
  (32 shorter events, 2.7 us)
Async XLA Ops:
  7.2 100.2 %all-gather.3.cloned.1.call-start = ((), (), s32[]{:S(2)}) async-start(), calls=%async_computation.6 | async-start | bytes 3440640 | tf_op jit(solution)/shard_map/all_gather | solution.py:68
  11.9 54.6 %all-to-all-start = ((bf16[4,3,64,1792]{3,2,1,0:T(8,128)(2,1)}), bf16[4,3,64,1792]{3,2,1,0:T(8,128)(2,1)S(1)}, u32[]{:S(2)}, u32[]{:S(2)}) async-start(bf16[4,3,64,1792]{3,2,1,0:T(8,128)(2,1)} %stack.2), calls=%async_computation | async-start | bytes 5505024 | tf_op jit(solution)/shard_map/all_to_all | solution.py:63
  18.5 2.4 copy-start
  18.5 179.4 %all-gather.5.cloned.1.call-start = ((), (), s32[]{:S(2)}) async-start(), calls=%async_computation.7 | async-start | bytes 3440640 | tf_op jit(solution)/shard_map/all_gather | solution.py:69
  86.5 7.7 %copy-start.1 = (s32[1,2048,2]{1,2,0:T(2,128)S(1)}, s32[1,2048,2]{1,2,0:T(2,128)}, u32[]{:S(2)}) copy-start(s32[1,2048,2]{1,2,0:T(2,128)} %param.12) | copy-start | bytes 49156
  86.5 43.5 %all-to-all-start.1 = ((bf16[32,2,21504]{2,1,0:T(2,128)(2,1)}), bf16[32,2,21504]{2,1,0:T(2,128)(2,1)S(1)}, u32[]{:S(2)}, u32[]{:S(2)}) async-start(bf16[32,2,21504]{2,1,0:T(2,128)(2,1)} %reshape.115), calls=%async_computation.1 | async-start | bytes 5505024 | tf_op jit(solution)/shard_map/all_to_all | solution.py:72
  130.0 42.7 %all-to-all-start.2 = ((bf16[32,2,21504]{2,1,0:T(2,128)(2,1)}), bf16[32,2,21504]{2,1,0:T(2,128)(2,1)}, u32[]{:S(2)}, u32[]{:S(2)}) async-start(bf16[32,2,21504]{2,1,0:T(2,128)(2,1)} %reshape.117), calls=%async_computation.2 | async-start | bytes 5505024 | tf_op jit(solution)/shard_map/all_to_all | solution.py:73
  137.9 199.5 %reduce-scatter.4.cloned.1.call-start = ((), (), s32[]{:S(2)}) async-start(), calls=%async_computation.8 | async-start | bytes 10485760 | tf_op jit(solution)/shard_map/reduce_scatter | solution.py:16
  156.4 8.3 %slice-start = ((s8[8388608]{0:T(1024)(128)(4,1)}), s8[4194304]{0:T(1024)(128)(4,1)S(1)}, s32[]{:S(2)}) async-start(s8[8388608]{0:T(1024)(128)(4,1)} %bitcast.54), calls=%async_computation.11 | async-start | bytes 8388608
  157.0 7.7 %slice-start.1 = ((s8[8388608]{0:T(1024)(128)(4,1)}), s8[4194304]{0:T(1024)(128)(4,1)S(1)}, s32[]{:S(2)}) async-start(s8[8388608]{0:T(1024)(128)(4,1)} %bitcast.54), calls=%async_computation.12 | async-start | bytes 8388608
  255.9 113.2 %reduce-scatter.6.cloned.1.call-start = ((), (), s32[]{:S(2)}) async-start(), calls=%async_computation.9 | async-start | bytes 2621440 | tf_op jit(solution)/shard_map/reduce_scatter | solution.py:16
  337.5 51.3 %reduce-scatter.8.cloned.1.call-start = ((), (), s32[]{:S(2)}) async-start(), calls=%async_computation.10 | async-start | bytes 786432 | tf_op jit(solution)/shard_map/reduce_scatter | solution.py:16
Sparse Core Ops, SparseCore 0:
  10.2 48.8 all-gather.2
  60.8 29.6 all-gather.4
  256.0 81.4 reduce-scatter.3
  339.7 29.3 reduce-scatter.5
  371.9 16.8 reduce-scatter.7
